TPU v7x, 32 devices: a whole 2x2x4 slice. The times are simulated.
32 devices in a mesh: sp: 16 (over z, y, x), tp: 2 (over core).
Axes of the slice: x: 2, y: 2, z: 4, core: 2. Of those that a mesh axis runs over, the one named last changes fastest.
Arguments:
- queries: bfloat16 [8192, 2048], P('sp', 'tp'), may hold values from -6 to 6
- keys: bfloat16 [8192, 1024], P('sp', 'tp'), may hold values from -6 to 6
- values: bfloat16 [8192, 1024], P('sp', 'tp'), may hold values from -6 to 6
- documents: int32 [8192], P('sp'), may hold values from 0 to 3, never falling along the last dimension, each value on 1 to 4096 neighbouring positions
- query_gain: float32 [128], replicated, may hold values from 1.8 to 6
- key_gain: float32 [128], replicated, may hold values from 1.8 to 6
- residual: bfloat16 [8192, 4096], P('sp', 'tp'), may hold values from -6 to 6
- out_weight: bfloat16 [2048, 4096], P('tp'), may hold values from -0.125 to 0.125
- norm_gain: float32 [4096], replicated, may hold values from 0.1 to 1.9
- up_weight: bfloat16 [4096, 16384], P('sp', 'tp'), may hold values from -0.09375 to 0.09375
- down_weight: bfloat16 [16384, 4096], P('tp', 'sp'), may hold values from -0.046875 to 0.046875
Outputs:
- mixed: bfloat16 [8192, 4096], P('sp', 'tp')
Inputs may be any that keep to these rules, and one draw needn't show every extreme that they name: `documents`: document numbers never fall along the sequence; a document has at most 4096 positions.
All inputs are finite; a program needn't handle non-finite values.
Results may differ from a plain program's by a relative error of at most 0.017.
The roundings to bfloat16 on the way count: a program that leaves them out, or rounds other values in their place, can miss the bound.
Values may be sent and summed in bfloat16 or wider, within the bound.
No kernel may reach another device: no remote copies, remote signals or barrier semaphores. Data moves between devices by JAX's collectives and lax.ppermute only.
A program may use at most 256 MiB of HBM per device.

v0:
```python
import jax
import jax.numpy as jnp
from jax import lax
from jax.sharding import PartitionSpec as P

HQ = 16
KV = 8
HD = 128
GRID_W = 64
norm_eps = 1e-06
rope_base = 10000.0
masked_score = -1e30


def head_norm(heads_in, gain):
    values32 = heads_in.astype(jnp.float32)
    scaled = values32 * lax.rsqrt(jnp.mean(values32 * values32, axis=-1, keepdims=True) + norm_eps)
    return scaled * gain


def rotate_half(heads_in, position):
    quarter = heads_in.shape[-1] // 2
    inverse_freq = rope_base ** (-jnp.arange(quarter, dtype=jnp.float32) / quarter)
    angles = position[:, None] * inverse_freq[None, :]
    cosine_part = jnp.cos(angles)[:, None, :]
    sine_part = jnp.sin(angles)[:, None, :]
    leading = heads_in[..., :quarter]
    trailing = heads_in[..., quarter:]
    return jnp.concatenate(
        [
            leading * cosine_part - trailing * sine_part,
            leading * sine_part + trailing * cosine_part,
        ],
        axis=-1,
    )


def grid_rotary(heads_in, positions):
    half_width = heads_in.shape[-1] // 2
    grid_row = (positions // GRID_W).astype(jnp.float32)
    grid_col = (positions % GRID_W).astype(jnp.float32)
    return jnp.concatenate(
        [
            rotate_half(heads_in[..., :half_width], grid_row),
            rotate_half(heads_in[..., half_width:], grid_col),
        ],
        axis=-1,
    )


def body(
    queries,
    keys,
    values,
    documents,
    query_gain,
    key_gain,
    residual,
    out_weight,
    norm_gain,
    up_weight,
    down_weight,
):
    tok_rows = queries.shape[0]
    key_heads = keys.shape[1] // HD
    group_size = HQ // KV
    width_local = residual.shape[1]
    tp_index = lax.axis_index("tp")
    up_whole, down_whole = (
        lax.all_gather(up_weight, "sp", axis=0, tiled=True),
        lax.all_gather(down_weight, "sp", axis=1, tiled=True),
    )
    residual_whole = lax.all_gather(residual, "tp", axis=1, tiled=True)
    positions = lax.axis_index("sp") * tok_rows + jnp.arange(tok_rows, dtype=jnp.int32)
    queries_rot = grid_rotary(
        head_norm(queries.reshape(tok_rows, key_heads * group_size, HD), query_gain), positions
    )
    queries_rot = queries_rot.astype(jnp.bfloat16).reshape(tok_rows, key_heads, group_size, HD)
    keys_rot = grid_rotary(
        head_norm(keys.reshape(tok_rows, key_heads, HD), key_gain), positions
    ).astype(jnp.bfloat16)
    value_heads = values.reshape(tok_rows, key_heads, HD)
    own_docs = documents.astype(jnp.bfloat16)
    score_scale = HD ** (-0.5)
    running_max = jnp.full((key_heads, group_size, tok_rows), masked_score, jnp.float32)
    key_piece = lax.all_gather(keys_rot, "sp", axis=0, tiled=True)
    value_piece = lax.all_gather(value_heads, "sp", axis=0, tiled=True)
    doc_piece = lax.all_gather(own_docs, "sp", axis=0, tiled=True)
    scores = (
        jnp.einsum("qkgd,skd->kgqs", queries_rot, key_piece, preferred_element_type=jnp.float32)
        * score_scale
    )
    same_doc = own_docs[:, None] == doc_piece[None, :]
    scores = jnp.where(same_doc, scores, masked_score)
    new_max = jnp.maximum(running_max, jnp.max(scores, axis=-1))
    probs = jnp.where(same_doc, jnp.exp(scores - new_max[..., None]), 0.0)
    running_sum = jnp.sum(probs, axis=-1)
    update = jnp.einsum(
        "kgqs,skd->qkgd",
        probs.astype(jnp.bfloat16),
        value_piece,
        preferred_element_type=jnp.float32,
    )
    weighted = update
    running_max, running_sum, weighted = (new_max, running_sum, weighted)
    attended = (weighted / jnp.transpose(running_sum, (2, 0, 1))[..., None]).astype(jnp.bfloat16)
    attended = attended.reshape(tok_rows, key_heads * group_size * HD)
    partial_out = jnp.dot(attended, out_weight, preferred_element_type=jnp.float32)
    branch = lax.psum(partial_out.astype(jnp.bfloat16), "tp").astype(jnp.float32)
    stream_whole = residual_whole.astype(jnp.float32) + branch
    normed = stream_whole * lax.rsqrt(
        jnp.mean(stream_whole * stream_whole, axis=-1, keepdims=True) + norm_eps
    )
    normed = (normed * norm_gain).astype(jnp.bfloat16)
    stream = lax.dynamic_slice_in_dim(stream_whole, tp_index * width_local, width_local, 1)
    hidden = jnp.dot(normed, up_whole, preferred_element_type=jnp.float32)
    positive = jnp.maximum(hidden, 0.0)
    squared = (positive * positive).astype(jnp.bfloat16)
    product = jnp.dot(squared, down_whole, preferred_element_type=jnp.float32)
    feed = lax.psum_scatter(
        product.astype(jnp.bfloat16), "tp", scatter_dimension=1, tiled=True
    ).astype(jnp.float32)
    return (stream + feed).astype(jnp.bfloat16)


def solution(mesh):
    in_specs = (
        P("sp", "tp"),
        P("sp", "tp"),
        P("sp", "tp"),
        P("sp"),
        P(),
        P(),
        P("sp", "tp"),
        P("tp", None),
        P(),
        P("sp", "tp"),
        P("tp", "sp"),
    )
    out_specs = P("sp", "tp")
    return jax.shard_map(body, mesh=mesh, in_specs=in_specs, out_specs=out_specs, check_vma=False)
```

profile of v0, /device:TPU:0, one launch (start us, length us, event | category | flops | bytes accessed | tf_op | source)
XLA Modules:
  0.0 2437.9 jit_solution(14920959515710849771)
XLA Ops:
  6.6 1.3 copy.28
  8.0 0.2 copy.29
  8.3 1.9 multiply_cosine_fusion.1
  10.1 1.0 multiply_multiply_fusion.1
  11.1 0.9 subtract_convert_fusion.3
  12.1 1.5 pad_maximum_fusion
  13.6 1.0 copy.36
  14.7 0.7 all-gather.7.cloned.1.call-update
  15.5 0.2 convert_bitcast_fusion
  15.7 0.5 copy.42
  16.2 0.6 multiply_reduce_fusion.1
  17.1 0.9 multiply_multiply_fusion
  18.0 1.8 subtract_convert_fusion.1
  20.2 1.1 copy.35
  21.4 54.7 %all-gather = bf16[16,1,512]{2,1,0:T(2,128)(2,1)S(1)} all-gather(bf16[1,1,512]{2,1,0:T(2,128)(2,1)S(1)} %reshape.192), channel_id=1, replica_groups=mesh['sp'=16,'tp'=2] {'sp'}, dimensions={0}, use_global_device_ids=true | all-gather | bytes 17408 | tf_op jit(solution)/shard_map/all_gather | solution.py:88
  76.2 4.0 broadcast_compare_fusion
  80.2 48.9 %all-gather.9.cloned.1.call-done = bf16[8192,4,128]{2,0,1:T(8,128)(2,1)} async-done(((bf16[512,4,128]{2,0,1:T(8,128)(2,1)}), bf16[8192,4,128]{2,0,1:T(8,128)(2,1)}) %all-gather.9.cloned.1.call-update) | async-done | bytes 8388624 | tf_op jit(solution)/shard_map/all_gather | solution.py:86
  129.1 52.2 %fusion = (f32[4,2,512]{2,1,0:T(2,128)S(1)}, f32[4,8192,512,2]{2,1,3,0:T(8,128)}) fusion(pred[512,8192]{0,1:T(8,128)(4,1)} %broadcast_compare_fusion, bf16[512,4,2,32]{3,0,2,1:T(8,128)(2,1)} %bitcast.60, bf16[512,4,2,32]{3,0,2,1:T(8,128)(2,1)S(1)} %bitcast.59, bf16[512,4,2,32]{3,0,2,1:T(8,128)(2,1)S(1)} %bitcast.58, ...), kind=kOutput, calls=%fused_computation.2 | convolution fusion | flops 8694788096 | bytes 147865600 | tf_op jit(solution)/shard_map/qkgd,skd->kgqs/dot_general | solution.py:90
  181.3 43.7 %fusion.1 = f32[4,2,512]{2,1,0:T(2,128)S(1)} fusion(f32[4,8192,512,2]{2,1,3,0:T(8,128)} %get-tuple-element.26, f32[4,2,512]{2,1,0:T(2,128)S(1)} %broadcast_maximum_fusion, pred[512,8192]{0,1:T(8,128)(4,1)} %broadcast_compare_fusion), kind=kLoop, calls=%fused_computation.3 | loop fusion | flops 167768064 | bytes 138444800 | tf_op jit(solution)/shard_map/reduce_sum | solution.py:97
  225.0 25.8 %all-gather.11.cloned.1.call-done = bf16[8192,4,128]{0,2,1:T(8,128)(2,1)} async-done(((bf16[512,4,128]{0,2,1:T(8,128)(2,1)}), bf16[8192,4,128]{0,2,1:T(8,128)(2,1)}) %all-gather.11.cloned.1.call-update) | async-done | bytes 8388624 | tf_op jit(solution)/shard_map/all_gather | solution.py:87
  250.7 51.7 %fusion.11 = bf16[512,4,2,128]{0,3,2,1:T(8,128)(2,1)S(1)} fusion(f32[4,8192,512,2]{2,1,3,0:T(8,128)} %get-tuple-element.26, f32[4,2,512]{2,1,0:T(2,128)S(1)} %broadcast_maximum_fusion, pred[512,8192]{0,1:T(8,128)(4,1)} %broadcast_compare_fusion, bf16[8192,4,128]{0,2,1:T(8,128)(2,1)} %all-gather.11.cloned.1.call-done, f32[512,4,2]{0,2,1:T(2,128)S(1)} %bitcast.63), kind=kOutput, calls=%fused_computation.21 | convolution fusion | flops 8758755328 | bytes 147881984 | tf_op jit(solution)/shard_map/kgqs,skd->qkgd/dot_general | solution.py:98
  302.5 9.5 convolution_convert_fusion.1
  312.1 0.5 all-gather.13.cloned.1.call-update
  312.7 0.5 all-gather.15.cloned.1.call-update
  313.3 25.2 %all-reduce.2.cloned.1.call-done = bf16[512,4096]{1,0:T(8,128)(2,1)} async-done(((bf16[512,4096]{1,0:T(8,128)(2,1)}), bf16[512,4096]{1,0:T(8,128)(2,1)}) %all-reduce.2.cloned.1.call-update) | async-done | bytes 4194320 | tf_op jit(solution)/shard_map/psum | solution.py:109
  338.4 8.0 convert_add_fusion
  346.5 663.9 %all-gather.13.cloned.1.call-done = bf16[4096,8192]{1,0:T(8,128)(2,1)} async-done(((bf16[256,8192]{1,0:T(8,128)(2,1)}), bf16[4096,8192]{1,0:T(8,128)(2,1)}) %all-gather.13.cloned.1.call-update) | async-done | bytes 67108880 | tf_op jit(solution)/shard_map/all_gather | solution.py:70
  1010.4 45.3 %multiply_convert_fusion = bf16[512,8192]{1,0:T(8,128)(2,1)} fusion(bf16[4096,8192]{1,0:T(8,128)(2,1)} %all-gather.13.cloned.1.call-done, f32[4096]{0:T(1024)S(1)} %copy-done.4, f32[512]{0:T(512)S(1)} %add_rsqrt_fusion.2, bf16[512,4096]{1,0:T(8,128)(2,1)} %all-reduce.2.cloned.1.call-done, bf16[512,4096]{1,0:T(8,128)(2,1)} %all-gather.7.cloned.1.call-done), kind=kOutput, calls=%fused_computation.7 | convolution fusion | flops 34384904192 | bytes 83904512 | tf_op jit(solution)/shard_map/dot_general | solution.py:116
  1055.7 1312.2 %all-gather.15.cloned.1.call-done = bf16[8192,4096]{1,0:T(8,128)(2,1)} async-done(((bf16[8192,256]{1,0:T(8,128)(2,1)}), bf16[8192,4096]{1,0:T(8,128)(2,1)}) %all-gather.15.cloned.1.call-update) | async-done | bytes 67108880 | tf_op jit(solution)/shard_map/all_gather | solution.py:71
  2368.0 44.5 %convolution_convert_fusion = bf16[512,4096]{1,0:T(8,128)(2,1)} fusion(bf16[512,8192]{1,0:T(8,128)(2,1)} %multiply_convert_fusion, bf16[8192,4096]{1,0:T(8,128)(2,1)} %all-gather.15.cloned.1.call-done), kind=kOutput, calls=%fused_computation.14 | convolution fusion | flops 34361835520 | bytes 79691776 | tf_op jit(solution)/shard_map/dot_general | solution.py:119
  2412.5 13.3 reduce-scatter.2.cloned.1.call-done
  2425.8 4.8 add_convert_fusion
  (38 shorter events, 1.3 us)
Async XLA Ops:
  6.5 122.5 %all-gather.9.cloned.1.call-start = ((), (), s32[]{:S(2)}) async-start(), calls=%async_computation.2 | async-start | bytes 8912896 | tf_op jit(solution)/shard_map/all_gather | solution.py:86
  6.6 7.0 copy-start.1
  11.1 4.3 copy-start
  12.0 5.1 copy-start.3
  13.6 237.2 %all-gather.11.cloned.1.call-start = ((), (), s32[]{:S(2)}) async-start(), calls=%async_computation.3 | async-start | bytes 8912896 | tf_op jit(solution)/shard_map/all_gather | solution.py:87
  14.7 298.6 %all-gather.7.cloned.1.call-start = ((), (), s32[]{:S(2)}) async-start(), calls=%async_computation.1 | async-start | bytes 6291456 | tf_op jit(solution)/shard_map/all_gather | solution.py:73
  15.4 323.0 %all-reduce.2.cloned.1.call-start = ((), (), s32[]{:S(2)}) async-start(), calls=%async_computation.4 | async-start | bytes 8388608 | tf_op jit(solution)/shard_map/psum | solution.py:109
  18.0 3.4 copy-start.2
  312.0 698.4 %all-gather.13.cloned.1.call-start = ((), (), s32[]{:S(2)}) async-start(), calls=%async_computation.5 | async-start | bytes 71303168 | tf_op jit(solution)/shard_map/all_gather | solution.py:70
  312.6 2055.4 %all-gather.15.cloned.1.call-start = ((), (), s32[]{:S(2)}) async-start(), calls=%async_computation.6 | async-start | bytes 71303168 | tf_op jit(solution)/shard_map/all_gather | solution.py:71
  313.2 697.2 %copy-start.4 = (f32[4096]{0:T(1024)S(1)}, f32[4096]{0:T(1024)}, u32[]{:S(2)}) copy-start(f32[4096]{0:T(1024)} %param.19) | copy-start | bytes 49156
  313.2 2112.6 %reduce-scatter.2.cloned.1.call-start = ((), (), s32[]{:S(2)}) async-start(), calls=%async_computation.7 | async-start | bytes 6291456 | tf_op jit(solution)/shard_map/reduce_scatter | solution.py:120
Sparse Core Ops, SparseCore 0:
  13.7 115.3 all-gather.8
  131.8 118.9 all-gather.10
  252.3 11.8 all-gather.6
  312.1 26.2 all-reduce.1
  341.1 669.3 all-gather.12
  1011.8 1356.1 all-gather.14
  2412.6 13.0 reduce-scatter.1
where the time goes:
time: 2440 us
  waiting for transfers between devices  2090 us (86%)
  matrix products  203 us (8%)
  other arithmetic  69.7 us (3%)
  blocking collectives  54.7 us (2%)
    all_gather x1, waiting for transfers between devices, body(): lax.all_gather(down_weight, 'sp', axis=1, tiled=True)  1310 us
    all_gather x1, waiting for transfers between devices, body(): lax.all_gather(up_weight, 'sp', axis=0, tiled=True)  664 us
    all_gather x1, blocking collectives, body(): doc_piece = lax.all_gather(own_docs, 'sp', axis=0, tiled=True)  54.7 us
    dot_general x1, matrix products, body(): jnp.einsum('qkgd,skd->kgqs', queries_rot, key_piece, preferred_element_ty...  52.2 us
    dot_general x1, matrix products, body(): jnp.einsum('kgqs,skd->qkgd', probs.astype(jnp.bfloat16), value_piece, pre...  51.7 us
    all_gather x1, waiting for transfers between devices, body(): key_piece = lax.all_gather(keys_rot, 'sp', axis=0, tiled=True)  48.9 us
  transfers between devices with their start and end apart: 7, of which 6 were waited for; matrix products, arithmetic and copies ran while one was open for 9% of the time, Pallas kernels for 0%

commit v1 on v0

--- a/solution.py
+++ b/solution.py
@@ -68,7 +68,7 @@
     tp_index = lax.axis_index("tp")
     up_whole, down_whole = (
         lax.all_gather(up_weight, "sp", axis=0, tiled=True),
-        lax.all_gather(down_weight, "sp", axis=1, tiled=True),
+        jnp.concatenate(lax.all_gather(down_weight, "sp"), axis=1),
     )
     residual_whole = lax.all_gather(residual, "tp", axis=1, tiled=True)
     positions = lax.axis_index("sp") * tok_rows + jnp.arange(tok_rows, dtype=jnp.int32)

time: 2440 us -> 1790 us (0.73)
  waiting for transfers between devices: 2090 us -> 1380 us
  local copies, waits for them, and re-layouts: 4.85 us -> 84.7 us
    all_gather x1, waiting for transfers between devices: 1310 us -> 664 us  [body(): lax.all_gather(down_weight, 'sp')]
    reshape x0 -> x1, local copies, waits for them, and re-layouts: none -> 79.9 us  [body(): jnp.concatenate(lax.all_gather(down_weight, 'sp'), axis=1)]
    all_gather x1, waiting for transfers between devices: 664 us -> 589 us  [body(): lax.all_gather(up_weight, 'sp', axis=0, tiled=True)]
  transfers between devices with their start and end apart: 7 -> 7, of which waited for: 6 -> 6; matrix products, arithmetic and copies ran while one was open for 9% -> 14% of each run, Pallas kernels for 0% -> 0%
where the time goes in v1:
time: 1790 us
  waiting for transfers between devices  1380 us (77%)
  matrix products  202 us (11%)
  local copies, waits for them, and re-layouts  84.7 us (5%)
  other arithmetic  69.7 us (4%)
  blocking collectives  43.8 us (2%)
    all_gather x1, waiting for transfers between devices, body(): lax.all_gather(down_weight, 'sp')  664 us
    all_gather x1, waiting for transfers between devices, body(): lax.all_gather(up_weight, 'sp', axis=0, tiled=True)  589 us
    reshape x1, local copies, waits for them, and re-layouts, body(): jnp.concatenate(lax.all_gather(down_weight, 'sp'), axis=1)  79.9 us
    all_gather x1, waiting for transfers between devices, body(): key_piece = lax.all_gather(keys_rot, 'sp', axis=0, tiled=True)  59.7 us
    dot_general x1, matrix products, body(): jnp.einsum('qkgd,skd->kgqs', queries_rot, key_piece, preferred_element_ty...  52.2 us
    dot_general x1, matrix products, body(): jnp.einsum('kgqs,skd->qkgd', probs.astype(jnp.bfloat16), value_piece, pre...  51.7 us
    dot_general x1, matrix products, body(): hidden = jnp.dot(normed, up_whole, preferred_element_type=jnp.float32)  45.1 us
    all_gather x1, blocking collectives, body(): doc_piece = lax.all_gather(own_docs, 'sp', axis=0, tiled=True)  43.8 us
  transfers between devices with their start and end apart: 7, of which 6 were waited for; matrix products, arithmetic and copies ran while one was open for 14% of the time, Pallas kernels for 0%

profile of v1, /device:TPU:0, one launch (start us, length us, event | category | flops | bytes accessed | tf_op | source)
XLA Modules:
  0.0 1789.6 jit_solution(14031028241657721471)
XLA Ops:
  6.6 1.3 copy.35
  8.3 1.9 multiply_cosine_fusion.1
  10.1 1.0 multiply_multiply_fusion.1
  11.1 0.9 subtract_convert_fusion.3
  12.1 1.5 pad_maximum_fusion
  13.6 1.0 copy.43
  14.7 0.7 all-gather.8.cloned.1.call-update
  15.4 0.2 convert_bitcast_fusion
  15.7 0.5 copy.50
  16.2 0.6 multiply_reduce_fusion.1
  17.1 0.9 multiply_multiply_fusion
  17.9 1.8 subtract_convert_fusion.1
  20.2 1.1 copy.42
  21.3 43.8 %all-gather.1 = bf16[16,1,512]{2,1,0:T(2,128)(2,1)S(1)} all-gather(bf16[1,1,512]{2,1,0:T(2,128)(2,1)S(1)} %reshape.201), channel_id=1, replica_groups=mesh['sp'=16,'tp'=2] {'sp'}, dimensions={0}, use_global_device_ids=true | all-gather | bytes 17408 | tf_op jit(solution)/shard_map/all_gather | solution.py:88
  65.2 4.1 broadcast_compare_fusion
  69.3 59.7 %all-gather.10.cloned.1.call-done = bf16[8192,4,128]{2,0,1:T(8,128)(2,1)} async-done(((bf16[512,4,128]{2,0,1:T(8,128)(2,1)}), bf16[8192,4,128]{2,0,1:T(8,128)(2,1)}) %all-gather.10.cloned.1.call-update) | async-done | bytes 8388624 | tf_op jit(solution)/shard_map/all_gather | solution.py:86
  129.0 52.2 %fusion = (f32[4,2,512]{2,1,0:T(2,128)S(1)}, f32[4,8192,512,2]{2,1,3,0:T(8,128)}) fusion(pred[512,8192]{0,1:T(8,128)(4,1)} %broadcast_compare_fusion, bf16[512,4,2,32]{3,0,2,1:T(8,128)(2,1)} %bitcast.68, bf16[512,4,2,32]{3,0,2,1:T(8,128)(2,1)S(1)} %bitcast.67, bf16[512,4,2,32]{3,0,2,1:T(8,128)(2,1)S(1)} %bitcast.66, ...), kind=kOutput, calls=%fused_computation.2 | convolution fusion | flops 8694788096 | bytes 147865600 | tf_op jit(solution)/shard_map/qkgd,skd->kgqs/dot_general | solution.py:90
  181.2 43.7 %fusion.1 = f32[4,2,512]{2,1,0:T(2,128)S(1)} fusion(f32[4,8192,512,2]{2,1,3,0:T(8,128)} %get-tuple-element.26, f32[4,2,512]{2,1,0:T(2,128)S(1)} %broadcast_maximum_fusion, pred[512,8192]{0,1:T(8,128)(4,1)} %broadcast_compare_fusion), kind=kLoop, calls=%fused_computation.3 | loop fusion | flops 167768064 | bytes 138444800 | tf_op jit(solution)/shard_map/reduce_sum | solution.py:97
  224.9 25.8 %all-gather.12.cloned.1.call-done = bf16[8192,4,128]{0,2,1:T(8,128)(2,1)} async-done(((bf16[512,4,128]{0,2,1:T(8,128)(2,1)}), bf16[8192,4,128]{0,2,1:T(8,128)(2,1)}) %all-gather.12.cloned.1.call-update) | async-done | bytes 8388624 | tf_op jit(solution)/shard_map/all_gather | solution.py:87
  250.6 51.7 %fusion.16 = bf16[512,4,2,128]{0,3,2,1:T(8,128)(2,1)S(1)} fusion(f32[4,8192,512,2]{2,1,3,0:T(8,128)} %get-tuple-element.26, f32[4,2,512]{2,1,0:T(2,128)S(1)} %broadcast_maximum_fusion, pred[512,8192]{0,1:T(8,128)(4,1)} %broadcast_compare_fusion, bf16[8192,4,128]{0,2,1:T(8,128)(2,1)} %all-gather.12.cloned.1.call-done, f32[512,4,2]{0,2,1:T(2,128)S(1)} %bitcast.71), kind=kOutput, calls=%fused_computation.23 | convolution fusion | flops 8758755328 | bytes 147881984 | tf_op jit(solution)/shard_map/kgqs,skd->qkgd/dot_general | solution.py:98
  302.4 9.8 convolution_convert_fusion
  312.2 0.5 all-gather.16.cloned.1.call-update
  312.8 0.5 all-gather.14.cloned.1.call-update
  313.4 25.3 %all-reduce.2.cloned.1.call-done = bf16[512,4096]{1,0:T(8,128)(2,1)} async-done(((bf16[512,4096]{1,0:T(8,128)(2,1)}), bf16[512,4096]{1,0:T(8,128)(2,1)}) %all-reduce.2.cloned.1.call-update) | async-done | bytes 4194320 | tf_op jit(solution)/shard_map/psum | solution.py:109
  338.7 8.0 convert_add_fusion
  346.8 663.9 %all-gather.16.cloned.1.call-done = bf16[131072,256]{1,0:T(8,128)(2,1)} async-done(((bf16[8192,256]{1,0:T(8,128)(2,1)}), bf16[131072,256]{1,0:T(8,128)(2,1)}) %all-gather.16.cloned.1.call-update) | async-done | bytes 67108880 | tf_op jit(solution)/shard_map/all_gather | solution.py:71
  1010.7 79.9 %copy.45 = bf16[8192,16,256]{0,2,1:T(8,128)(2,1)} copy(bf16[8192,16,256]{2,0,1:T(8,128)(2,1)} %bitcast.16) | data formatting | bytes 134217728 | tf_op jit(solution)/shard_map/reshape | solution.py:71
  1090.6 589.1 %all-gather.14.cloned.1.call-done = bf16[4096,8192]{1,0:T(8,128)(2,1)} async-done(((bf16[256,8192]{1,0:T(8,128)(2,1)}), bf16[4096,8192]{1,0:T(8,128)(2,1)}) %all-gather.14.cloned.1.call-update) | async-done | bytes 67108880 | tf_op jit(solution)/shard_map/all_gather | solution.py:70
  1679.7 45.1 %multiply_convert_fusion.clone.6 = bf16[512,8192]{1,0:T(8,128)(2,1)} fusion(bf16[4096,8192]{1,0:T(8,128)(2,1)} %all-gather.14.cloned.1.call-done, f32[4096]{0:T(1024)S(1)} %copy-done.4, f32[512]{0:T(512)S(1)} %add_rsqrt_fusion.2, bf16[512,4096]{1,0:T(8,128)(2,1)} %all-reduce.2.cloned.1.call-done, ...), kind=kOutput, calls=%fused_computation.7.clone.clone.clone.clone.clone.1 | convolution fusion | flops 34384904192 | bytes 83904512 | tf_op jit(solution)/shard_map/dot_general | solution.py:116
  1724.8 42.9 %fusion.11 = bf16[512,4096]{1,0:T(8,128)(2,1)} fusion(bf16[8192,4096]{0,1:T(8,128)(2,1)} %bitcast.17, bf16[512,8192]{1,0:T(8,128)(2,1)} %multiply_convert_fusion.clone.6), kind=kOutput, calls=%fused_computation.17 | convolution fusion | flops 34361835520 | bytes 79691776 | tf_op jit(solution)/shard_map/dot_general | solution.py:119
  1767.7 10.2 reduce-scatter.2.cloned.1.call-done
  1778.0 4.8 add_convert_fusion
  (39 shorter events, 1.5 us)
Async XLA Ops:
  6.5 122.4 %all-gather.10.cloned.1.call-start = ((), (), s32[]{:S(2)}) async-start(), calls=%async_computation.2 | async-start | bytes 8912896 | tf_op jit(solution)/shard_map/all_gather | solution.py:86
  6.6 7.0 copy-start.1
  11.1 4.3 copy-start
  12.0 5.0 copy-start.3
  13.6 237.1 %all-gather.12.cloned.1.call-start = ((), (), s32[]{:S(2)}) async-start(), calls=%async_computation.3 | async-start | bytes 8912896 | tf_op jit(solution)/shard_map/all_gather | solution.py:87
  14.7 298.7 %all-gather.8.cloned.1.call-start = ((), (), s32[]{:S(2)}) async-start(), calls=%async_computation.1 | async-start | bytes 6291456 | tf_op jit(solution)/shard_map/all_gather | solution.py:73
  15.4 323.3 %all-reduce.2.cloned.1.call-start = ((), (), s32[]{:S(2)}) async-start(), calls=%async_computation.4 | async-start | bytes 8388608 | tf_op jit(solution)/shard_map/psum | solution.py:109
  17.9 3.4 copy-start.2
  312.2 698.6 %all-gather.16.cloned.1.call-start = ((), (), s32[]{:S(2)}) async-start(), calls=%async_computation.7 | async-start | bytes 71303168 | tf_op jit(solution)/shard_map/all_gather | solution.py:71
  312.7 1367.0 %all-gather.14.cloned.1.call-start = ((), (), s32[]{:S(2)}) async-start(), calls=%async_computation.5 | async-start | bytes 71303168 | tf_op jit(solution)/shard_map/all_gather | solution.py:70
  313.3 1464.6 %reduce-scatter.2.cloned.1.call-start = ((), (), s32[]{:S(2)}) async-start(), calls=%async_computation.6 | async-start | bytes 6291456 | tf_op jit(solution)/shard_map/reduce_scatter | solution.py:120
  1010.7 669.0 %copy-start.4 = (f32[4096]{0:T(1024)S(1)}, f32[4096]{0:T(1024)}, u32[]{:S(2)}) copy-start(f32[4096]{0:T(1024)} %param.19) | copy-start | bytes 49156
Sparse Core Ops, SparseCore 0:
  13.7 115.2 all-gather.9
  131.7 118.9 all-gather.11
  252.2 11.8 all-gather.7
  312.3 26.4 all-reduce.1
  341.4 669.3 all-gather.15
  1013.4 666.3 all-gather.13
  1767.8 10.0 reduce-scatter.1
